TPU v7x, 32 devices: a whole 2x2x4 slice. The times are simulated.
32 devices in a mesh: grp: 2 (over y), fs: 4 (over z), tp: 4 (over x, core).
Axes of the slice: x: 2, y: 2, z: 4, core: 2. Of those that a mesh axis runs over, the one named last changes fastest.
Arguments:
- tokens: bfloat16 [3072, 2048], P(('grp', 'fs'), 'tp'), parts along dimension 0, may hold values from -6 to 6
- mix_gain: float32 [2048], replicated, may hold values from 0.1 to 1.9
- w_signal: bfloat16 [2048, 1024], P('fs', 'tp'), may hold values from -0.125 to 0.125
- w_outer_gate: bfloat16 [2048, 1024], P('fs', 'tp'), may hold values from -0.125 to 0.125
- w_inner_gate: bfloat16 [2048, 1024], P('fs', 'tp'), may hold values from -0.125 to 0.125
- mix_taps: float32 [3, 1024], P(None, 'tp'), may hold values from -3 to 3
- w_mix_out: bfloat16 [1024, 2048], P('tp', 'fs'), may hold values from -0.1875 to 0.1875
- ffn_gain: float32 [2048], replicated, may hold values from 0.1 to 1.9
- w_gate: bfloat16 [2048, 5120], P('fs', 'tp'), may hold values from -0.125 to 0.125
- w_value: bfloat16 [2048, 5120], P('fs', 'tp'), may hold values from -0.125 to 0.125
- up_taps: float32 [2, 3, 5120], P(None, None, 'tp'), may hold values from -3 to 3
- up_bias: float32 [2, 5120], P(None, 'tp'), may hold values from -3 to 3
- w_down: bfloat16 [5120, 2048], P('tp', 'fs'), may hold values from -0.078125 to 0.078125
Outputs:
- layer_out: bfloat16 [3072, 2048], P(('grp', 'fs'), 'tp'), parts along dimension 0
There are 2 independent parts, one for each index of `grp`. A program takes and returns all parts, laid end to end along the dimension named above; an argument that names none is the same for every part. Nothing has to cross between parts.
All inputs are finite; a program needn't handle non-finite values.
Results may differ from a plain program's by a relative error of at most 0.022.
Values may be sent and summed in bfloat16 or wider, within the bound.
A program may use at most 64 MiB of HBM per device.

v0:
```python
import jax
import jax.numpy as jnp
from jax import lax
from jax.sharding import PartitionSpec as P

SEQS_DEV = 2


def conv_positions(values, taps):
    width = values.shape[1]
    blocks = values.reshape(SEQS_DEV, -1, width)
    length = blocks.shape[1]
    padded = jnp.pad(blocks, ((0, 0), (2, 0), (0, 0)))
    result = (
        padded[:, 0:length] * taps[0]
        + padded[:, 1 : length + 1] * taps[1]
        + padded[:, 2 : length + 2] * taps[2]
    )
    return result.reshape(-1, width)


def rms_norm(stream, gain):
    values = stream.astype(jnp.float32)
    scale = lax.rsqrt(jnp.mean(values * values, axis=-1, keepdims=True) + 1e-06)
    return (values * scale * gain).astype(jnp.bfloat16)


def on_device(
    tokens,
    mix_gain,
    w_signal,
    w_outer_gate,
    w_inner_gate,
    mix_taps,
    w_mix_out,
    ffn_gain,
    w_gate,
    w_value,
    up_taps,
    up_bias,
    w_down,
):
    whole = lax.all_gather(tokens, "tp", axis=1, tiled=True)
    normed = rms_norm(whole, mix_gain)
    pieces = (
        lax.all_gather(w_signal, "fs", axis=0, tiled=True),
        lax.all_gather(w_outer_gate, "fs", axis=0, tiled=True),
        lax.all_gather(w_inner_gate, "fs", axis=0, tiled=True),
    )
    columns = normed
    signal, outer, inner = tuple(
        (jnp.dot(columns, piece, preferred_element_type=jnp.float32) for piece in pieces)
    )
    signal = signal.astype(jnp.bfloat16).astype(jnp.float32)
    outer = outer.astype(jnp.bfloat16).astype(jnp.float32)
    inner = inner.astype(jnp.bfloat16).astype(jnp.float32)
    mixed = (outer * conv_positions(inner * signal, mix_taps)).astype(jnp.bfloat16)
    mix_terms = jnp.dot(
        mixed,
        lax.all_gather(w_mix_out, "fs", axis=1, tiled=True),
        preferred_element_type=jnp.float32,
    )
    mix_sum = lax.psum_scatter(
        mix_terms.astype(jnp.bfloat16), "tp", scatter_dimension=1, tiled=True
    ).astype(jnp.float32)
    resid = (tokens.astype(jnp.float32) + mix_sum).astype(jnp.bfloat16)
    whole_ffn = lax.all_gather(resid, "tp", axis=1, tiled=True)
    normed_ffn = rms_norm(whole_ffn, ffn_gain)
    pieces = (
        lax.all_gather(w_gate, "fs", axis=0, tiled=True),
        lax.all_gather(w_value, "fs", axis=0, tiled=True),
    )
    columns = normed_ffn
    gate = jnp.dot(columns, pieces[0], preferred_element_type=jnp.float32)
    value = jnp.dot(columns, pieces[1], preferred_element_type=jnp.float32)
    gate = gate.astype(jnp.bfloat16).astype(jnp.float32)
    value = value.astype(jnp.bfloat16).astype(jnp.float32)
    gate_conv = conv_positions(gate, up_taps[0]) + up_bias[0]
    value_conv = conv_positions(value, up_taps[1]) + up_bias[1]
    hidden = (jax.nn.silu(gate_conv) * value_conv).astype(jnp.bfloat16)
    ffn_terms = jnp.dot(
        hidden, lax.all_gather(w_down, "fs", axis=1, tiled=True), preferred_element_type=jnp.float32
    )
    ffn_sum = lax.psum_scatter(
        ffn_terms.astype(jnp.bfloat16), "tp", scatter_dimension=1, tiled=True
    ).astype(jnp.float32)
    return (resid.astype(jnp.float32) + ffn_sum).astype(jnp.bfloat16)


def solution(mesh):
    placed = (
        P(("grp", "fs"), "tp"),
        P(),
        P("fs", "tp"),
        P("fs", "tp"),
        P("fs", "tp"),
        P(None, "tp"),
        P("tp", "fs"),
        P(),
        P("fs", "tp"),
        P("fs", "tp"),
        P(None, None, "tp"),
        P(None, "tp"),
        P("tp", "fs"),
    )
    return jax.shard_map(
        on_device, mesh=mesh, in_specs=placed, out_specs=P(("grp", "fs"), "tp"), check_vma=False
    )
```

profile of v0, /device:TPU:0, one launch (start us, length us, event | category | flops | bytes accessed | tf_op | source)
XLA Modules:
  0.0 537.4 jit_solution(5827497235861300328)
XLA Ops:
  6.5 0.7 all-gather.10.cloned.1.call-update
  7.3 0.7 all-gather.14.cloned.1.call-update
  8.1 0.7 all-gather.16.cloned.1.call-update
  9.4 0.5 all-gather.18.cloned.1.call-update
  10.0 0.8 fusion.32
  10.8 20.5 %all-gather.10.cloned.1.call-done = bf16[384,2048]{1,0:T(8,128)(2,1)} async-done(((bf16[384,512]{1,0:T(8,128)(2,1)}), bf16[384,2048]{1,0:T(8,128)(2,1)}) %all-gather.10.cloned.1.call-update) | async-done | bytes 1572880 | tf_op jit(solution)/shard_map/all_gather | solution.py:43
  31.3 1.8 fusion
  33.1 27.8 %all-gather.14.cloned.1.call-done = bf16[2048,256]{1,0:T(8,128)(2,1)} async-done(((bf16[512,256]{1,0:T(8,128)(2,1)}), bf16[2048,256]{1,0:T(8,128)(2,1)}) %all-gather.14.cloned.1.call-update) | async-done | bytes 1048592 | tf_op jit(solution)/shard_map/all_gather | solution.py:48
  60.9 2.3 fusion.18
  63.2 26.6 %all-gather.16.cloned.1.call-done = bf16[2048,256]{1,0:T(8,128)(2,1)} async-done(((bf16[512,256]{1,0:T(8,128)(2,1)}), bf16[2048,256]{1,0:T(8,128)(2,1)}) %all-gather.16.cloned.1.call-update) | async-done | bytes 1048592 | tf_op jit(solution)/shard_map/all_gather | solution.py:46
  89.8 1.8 fusion.17
  91.8 26.8 %all-gather.12.cloned.1.call-done = bf16[2048,256]{1,0:T(8,128)(2,1)} async-done(((bf16[512,256]{1,0:T(8,128)(2,1)}), bf16[2048,256]{1,0:T(8,128)(2,1)}) %all-gather.12.cloned.1.call-update) | async-done | bytes 1048592 | tf_op jit(solution)/shard_map/all_gather | solution.py:47
  118.6 28.8 %all-gather.18.cloned.1.call-done = bf16[256,2048]{1,0:T(8,128)(2,1)} async-done(((bf16[256,512]{1,0:T(8,128)(2,1)}), bf16[256,2048]{1,0:T(8,128)(2,1)}) %all-gather.18.cloned.1.call-update) | async-done | bytes 1048592 | tf_op jit(solution)/shard_map/all_gather | solution.py:60
  147.5 4.6 convolution_convert_fusion.3
  152.1 27.5 %reduce-scatter.3.cloned.1.call-done = bf16[384,512]{1,0:T(8,128)(2,1)} async-done(((bf16[384,2048]{1,0:T(8,128)(2,1)}), bf16[384,512]{1,0:T(8,128)(2,1)}) %reduce-scatter.3.cloned.1.call-update) | async-done | bytes 393232 | tf_op jit(solution)/shard_map/reduce_scatter | solution.py:63
  179.6 1.8 add_convert_fusion.1
  181.6 0.7 all-gather.24.cloned.1.call-update
  182.3 0.7 all-gather.22.cloned.1.call-update
  183.1 0.5 all-gather.26.cloned.1.call-update
  183.7 0.7 slice_reduce_fusion.7
  184.4 16.9 %all-gather.20.cloned.1.call-done = bf16[384,2048]{1,0:T(8,128)(2,1)} async-done(((bf16[384,512]{1,0:T(8,128)(2,1)}), bf16[384,2048]{1,0:T(8,128)(2,1)}) %all-gather.20.cloned.1.call-update) | async-done | bytes 1572880 | tf_op jit(solution)/shard_map/all_gather | solution.py:67
  201.3 1.8 fusion.3
  203.1 97.8 %all-gather.24.cloned.1.call-done = bf16[2048,1280]{1,0:T(8,128)(2,1)} async-done(((bf16[512,1280]{1,0:T(8,128)(2,1)}), bf16[2048,1280]{1,0:T(8,128)(2,1)}) %all-gather.24.cloned.1.call-update) | async-done | bytes 5242896 | tf_op jit(solution)/shard_map/all_gather | solution.py:71
  300.9 5.2 convolution_convert_fusion.1
  306.3 92.6 %all-gather.22.cloned.1.call-done = bf16[2048,1280]{1,0:T(8,128)(2,1)} async-done(((bf16[512,1280]{1,0:T(8,128)(2,1)}), bf16[2048,1280]{1,0:T(8,128)(2,1)}) %all-gather.22.cloned.1.call-update) | async-done | bytes 5242896 | tf_op jit(solution)/shard_map/all_gather | solution.py:70
  398.9 4.8 convolution_convert_fusion.2
  404.4 1.2 fusion.8
  405.6 0.6 fusion.15
  406.2 90.5 %all-gather.26.cloned.1.call-done = bf16[1280,2048]{1,0:T(8,128)(2,1)} async-done(((bf16[1280,512]{1,0:T(8,128)(2,1)}), bf16[1280,2048]{1,0:T(8,128)(2,1)}) %all-gather.26.cloned.1.call-update) | async-done | bytes 5242896 | tf_op jit(solution)/shard_map/all_gather | solution.py:82
  496.7 5.9 %convolution_convert_fusion = bf16[384,2048]{1,0:T(8,128)(2,1)} fusion(bf16[384,1280]{1,0:T(8,128)(2,1)S(1)} %fusion.15, bf16[1280,2048]{1,0:T(8,128)(2,1)} %all-gather.26.cloned.1.call-done), kind=kOutput, calls=%fused_computation.10 | convolution fusion | flops 2014052352 | bytes 7798784 | tf_op jit(solution)/shard_map/dot_general | solution.py:81
  502.6 26.5 %reduce-scatter.5.cloned.1.call-done = bf16[384,512]{1,0:T(8,128)(2,1)} async-done(((bf16[384,2048]{1,0:T(8,128)(2,1)}), bf16[384,512]{1,0:T(8,128)(2,1)}) %reduce-scatter.5.cloned.1.call-update) | async-done | bytes 393232 | tf_op jit(solution)/shard_map/reduce_scatter | solution.py:84
  529.1 1.8 add_convert_fusion
  (51 shorter events, 2.0 us)
Async XLA Ops:
  6.5 54.3 %copy-start.13 = (f32[2048]{0:T(1024)S(1)}, f32[2048]{0:T(1024)}, u32[]{:S(2)}) copy-start(f32[2048]{0:T(1024)} %param.14) | copy-start | bytes 24580
  6.5 24.7 %all-gather.10.cloned.1.call-start = ((), (), s32[]{:S(2)}) async-start(), calls=%async_computation.2 | async-start | bytes 1966080 | tf_op jit(solution)/shard_map/all_gather | solution.py:43
  7.3 53.6 %all-gather.14.cloned.1.call-start = ((), (), s32[]{:S(2)}) async-start(), calls=%async_computation.4 | async-start | bytes 1310720 | tf_op jit(solution)/shard_map/all_gather | solution.py:48
  8.0 81.8 %all-gather.16.cloned.1.call-start = ((), (), s32[]{:S(2)}) async-start(), calls=%async_computation.5 | async-start | bytes 1310720 | tf_op jit(solution)/shard_map/all_gather | solution.py:46
  8.7 109.9 %all-gather.12.cloned.1.call-start = ((), (), s32[]{:S(2)}) async-start(), calls=%async_computation.3 | async-start | bytes 1310720 | tf_op jit(solution)/shard_map/all_gather | solution.py:47
  9.3 138.1 %all-gather.18.cloned.1.call-start = ((), (), s32[]{:S(2)}) async-start(), calls=%async_computation.6 | async-start | bytes 1310720 | tf_op jit(solution)/shard_map/all_gather | solution.py:60
  9.9 169.7 %reduce-scatter.3.cloned.1.call-start = ((), (), s32[]{:S(2)}) async-start(), calls=%async_computation.7 | async-start | bytes 1966080 | tf_op jit(solution)/shard_map/reduce_scatter | solution.py:63
  33.1 56.8 %copy-start.1 = (bf16[384,2048]{1,0:T(8,128)(2,1)S(1)}, bf16[384,2048]{1,0:T(8,128)(2,1)}, u32[]{:S(2)}) copy-start(bf16[384,2048]{1,0:T(8,128)(2,1)} %all-gather.10.cloned.1.call-done) | copy-start | bytes 4718596
  147.5 32.2 %copy-start.3 = (bf16[384,512]{1,0:T(8,128)(2,1)S(1)}, bf16[384,512]{1,0:T(8,128)(2,1)}, u32[]{:S(2)}) copy-start(bf16[384,512]{1,0:T(8,128)(2,1)} %param.13) | copy-start | bytes 1179652
  152.1 49.2 %all-gather.20.cloned.1.call-start = ((), (), s32[]{:S(2)}) async-start(), calls=%async_computation.8 | async-start | bytes 1966080 | tf_op jit(solution)/shard_map/all_gather | solution.py:67
  181.5 2.2 copy-start.11
  181.5 2.2 copy-start.10
  181.5 119.4 %all-gather.24.cloned.1.call-start = ((), (), s32[]{:S(2)}) async-start(), calls=%async_computation.10 | async-start | bytes 6553600 | tf_op jit(solution)/shard_map/all_gather | solution.py:71
  182.3 118.7 %copy-start.14 = (f32[2048]{0:T(1024)S(1)}, f32[2048]{0:T(1024)}, u32[]{:S(2)}) copy-start(f32[2048]{0:T(1024)} %param.20) | copy-start | bytes 24580
  182.3 216.6 %all-gather.22.cloned.1.call-start = ((), (), s32[]{:S(2)}) async-start(), calls=%async_computation.9 | async-start | bytes 6553600 | tf_op jit(solution)/shard_map/all_gather | solution.py:70
  183.0 313.7 %all-gather.26.cloned.1.call-start = ((), (), s32[]{:S(2)}) async-start(), calls=%async_computation.11 | async-start | bytes 6553600 | tf_op jit(solution)/shard_map/all_gather | solution.py:82
  183.6 345.5 %reduce-scatter.5.cloned.1.call-start = ((), (), s32[]{:S(2)}) async-start(), calls=%async_computation.12 | async-start | bytes 1966080 | tf_op jit(solution)/shard_map/reduce_scatter | solution.py:84
  203.1 103.1 %copy-start.12 = (f32[384]{0:T(512)}, f32[384]{0:T(512)S(1)}, u32[]{:S(2)}) copy-start(f32[384]{0:T(512)S(1)} %add_rsqrt_fusion) | copy-start | bytes 4612
  306.1 92.8 %copy-start.2 = (bf16[384,2048]{1,0:T(8,128)(2,1)S(1)}, bf16[384,2048]{1,0:T(8,128)(2,1)}, u32[]{:S(2)}) copy-start(bf16[384,2048]{1,0:T(8,128)(2,1)} %all-gather.20.cloned.1.call-done) | copy-start | bytes 4718596
  403.7 0.7 copy-start.4
  403.7 0.7 copy-start.5
  403.7 0.7 copy-start.6
  403.7 0.7 copy-start.7
  403.7 0.7 copy-start.8
  403.7 0.7 copy-start.9
  406.2 122.9 %copy-start = (bf16[384,512]{1,0:T(8,128)(2,1)S(1)}, bf16[384,512]{1,0:T(8,128)(2,1)}, u32[]{:S(2)}) copy-start(bf16[384,512]{1,0:T(8,128)(2,1)} %add_convert_fusion.1) | copy-start | bytes 1179652
Sparse Core Ops, SparseCore 0:
  8.9 22.3 all-gather.9
  32.8 27.9 all-gather.13
  62.4 27.3 all-gather.15
  91.3 27.3 all-gather.11
  120.1 27.3 all-gather.17
  152.2 27.3 reduce-scatter.2
  181.6 19.6 all-gather.19
  202.8 98.0 all-gather.23
  302.5 96.3 all-gather.21
  400.3 96.3 all-gather.25
  502.7 26.3 reduce-scatter.4
where the time goes:
time: 538 us; the launch traced here: 537 us
  waiting for transfers between devices  488 us (91%)
  matrix products  24.6 us (5%)
  between operations  13.4 us (2%)
  other arithmetic  9.39 us (2%)
    all_gather x1, waiting for transfers between devices, on_device(): lax.all_gather(w_value, 'fs', axis=0, tiled=True)  97.8 us
    all_gather x1, waiting for transfers between devices, on_device(): lax.all_gather(w_gate, 'fs', axis=0, tiled=True)  92.6 us
    all_gather x1, waiting for transfers between devices, on_device(): lax.all_gather(w_down, 'fs', axis=1, tiled=True)  90.5 us
    all_gather x1, waiting for transfers between devices, on_device(): lax.all_gather(w_mix_out, 'fs', axis=1, tiled=True)  28.8 us
    all_gather x1, waiting for transfers between devices, on_device(): lax.all_gather(w_inner_gate, 'fs', axis=0, tiled=True)  27.8 us
    reduce_scatter x1, waiting for transfers between devices, on_device(): lax.psum_scatter(mix_terms.astype(jnp.bfloat16), 'tp', scatter_dimension=...  27.5 us
    all_gather x1, waiting for transfers between devices, on_device(): lax.all_gather(w_outer_gate, 'fs', axis=0, tiled=True)  26.8 us
    all_gather x1, waiting for transfers between devices, on_device(): lax.all_gather(w_signal, 'fs', axis=0, tiled=True)  26.6 us
  transfers between devices with their start and end apart: 11, of which 11 were waited for; matrix products, arithmetic and copies ran while one was open for 4% of the time, Pallas kernels for 0%

commit v1 on v0

--- a/solution.py
+++ b/solution.py
@@ -45,7 +45,9 @@
     pieces = (
         lax.all_gather(w_signal, "fs", axis=0, tiled=True),
         lax.all_gather(w_outer_gate, "fs", axis=0, tiled=True),
-        lax.all_gather(w_inner_gate, "fs", axis=0, tiled=True),
+        jnp.concatenate(
+            lax.all_to_all(jnp.stack([w_inner_gate] * lax.axis_size("fs")), "fs", 0, 0), axis=0
+        ),
     )
     columns = normed
     signal, outer, inner = tuple(

time: 538 us -> 510 us (0.948)
  waiting for transfers between devices: 488 us -> 451 us
  starting transfers between devices: 0.39 us -> 6.79 us
    all_gather x1 -> x0, waiting for transfers between devices: 27.8 us -> none  [on_device(): lax.all_gather(w_inner_gate, 'fs', axis=0, tiled=True)]
    all_gather x1, waiting for transfers between devices: 26.6 us -> 15.7 us  [on_device(): lax.all_gather(w_signal, 'fs', axis=0, tiled=True)]
    all_to_all x0 -> x1, waiting for transfers between devices: none -> 9.89 us  [on_device(): lax.all_to_all(jnp.stack([w_inner_gate] * lax.axis_size('fs')), 'fs', 0, 0)]
    all_gather x1, waiting for transfers between devices: 20.5 us -> 13.4 us  [on_device(): whole = lax.all_gather(tokens, 'tp', axis=1, tiled=True)]
    all_to_all x0 -> x1, starting transfers between devices: none -> 6.48 us  [on_device(): lax.all_to_all(jnp.stack([w_inner_gate] * lax.axis_size('fs')), 'fs', 0, 0)]
where the time goes in v1:
time: 510 us; the launch traced here: 509 us
  waiting for transfers between devices  451 us (88%)
  matrix products  24.4 us (5%)
  between operations  13.7 us (3%)
  other arithmetic  9.38 us (2%)
  starting transfers between devices  6.79 us (1%)
    all_gather x1, waiting for transfers between devices, on_device(): lax.all_gather(w_value, 'fs', axis=0, tiled=True)  97.8 us
    all_gather x1, waiting for transfers between devices, on_device(): lax.all_gather(w_gate, 'fs', axis=0, tiled=True)  92.6 us
    all_gather x1, waiting for transfers between devices, on_device(): lax.all_gather(w_down, 'fs', axis=1, tiled=True)  90.7 us
    all_gather x1, waiting for transfers between devices, on_device(): lax.all_gather(w_mix_out, 'fs', axis=1, tiled=True)  28.8 us
    reduce_scatter x1, waiting for transfers between devices, on_device(): lax.psum_scatter(mix_terms.astype(jnp.bfloat16), 'tp', scatter_dimension=...  27.5 us
    all_gather x1, waiting for transfers between devices, on_device(): lax.all_gather(w_outer_gate, 'fs', axis=0, tiled=True)  27 us
    reduce_scatter x1, waiting for transfers between devices, on_device(): lax.psum_scatter(ffn_terms.astype(jnp.bfloat16), 'tp', scatter_dimension=...  26.5 us
    all_gather x1, waiting for transfers between devices, on_device(): whole_ffn = lax.all_gather(resid, 'tp', axis=1, tiled=True)  16.7 us
  transfers between devices with their start and end apart: 11, of which 11 were waited for; matrix products, arithmetic and copies ran while one was open for 4% of the time, Pallas kernels for 0%

profile of v1, /device:TPU:0, one launch (start us, length us, event | category | flops | bytes accessed | tf_op | source)
XLA Modules:
  0.0 509.1 jit_solution(11357916685845319055)
XLA Ops:
  6.5 0.7 all-gather.9.cloned.1.call-update
  7.3 0.7 all-gather.13.cloned.1.call-update
  8.1 0.7 all-gather.11.cloned.1.call-update
  8.8 2.0 stack.2
  10.8 6.5 %all-to-all-start = ((bf16[4,512,256]{2,1,0:T(8,128)(2,1)}), bf16[4,512,256]{2,1,0:T(8,128)(2,1)S(1)}, u32[]{:S(2)}, u32[]{:S(2)}) async-start(bf16[4,512,256]{2,1,0:T(8,128)(2,1)} %stack.2), calls=%async_computation | async-start | bytes 2097152 | tf_op jit(solution)/shard_map/all_to_all | solution.py:49
  17.9 13.4 %all-gather.9.cloned.1.call-done = bf16[384,2048]{1,0:T(8,128)(2,1)} async-done(((bf16[384,512]{1,0:T(8,128)(2,1)}), bf16[384,2048]{1,0:T(8,128)(2,1)}) %all-gather.9.cloned.1.call-update) | async-done | bytes 1572880 | tf_op jit(solution)/shard_map/all_gather | solution.py:43
  31.3 1.8 fusion
  33.1 9.9 %all-to-all-done = bf16[4,512,256]{2,1,0:T(8,128)(2,1)S(1)} async-done(((bf16[4,512,256]{2,1,0:T(8,128)(2,1)}), bf16[4,512,256]{2,1,0:T(8,128)(2,1)S(1)}, u32[]{:S(2)}, u32[]{:S(2)}) %all-to-all-start) | async-done | bytes 1048608 | tf_op jit(solution)/shard_map/all_to_all | solution.py:49
  43.0 2.1 fusion.18
  45.1 15.7 %all-gather.13.cloned.1.call-done = bf16[2048,256]{1,0:T(8,128)(2,1)} async-done(((bf16[512,256]{1,0:T(8,128)(2,1)}), bf16[2048,256]{1,0:T(8,128)(2,1)}) %all-gather.13.cloned.1.call-update) | async-done | bytes 1048592 | tf_op jit(solution)/shard_map/all_gather | solution.py:46
  60.9 1.8 fusion.17
  62.8 27.0 %all-gather.11.cloned.1.call-done = bf16[2048,256]{1,0:T(8,128)(2,1)} async-done(((bf16[512,256]{1,0:T(8,128)(2,1)}), bf16[2048,256]{1,0:T(8,128)(2,1)}) %all-gather.11.cloned.1.call-update) | async-done | bytes 1048592 | tf_op jit(solution)/shard_map/all_gather | solution.py:47
  89.8 28.8 %all-gather.15.cloned.1.call-done = bf16[256,2048]{1,0:T(8,128)(2,1)} async-done(((bf16[256,512]{1,0:T(8,128)(2,1)}), bf16[256,2048]{1,0:T(8,128)(2,1)}) %all-gather.15.cloned.1.call-update) | async-done | bytes 1048592 | tf_op jit(solution)/shard_map/all_gather | solution.py:62
  118.7 4.6 convolution_convert_fusion.3
  123.3 27.5 %reduce-scatter.3.cloned.1.call-done = bf16[384,512]{1,0:T(8,128)(2,1)} async-done(((bf16[384,2048]{1,0:T(8,128)(2,1)}), bf16[384,512]{1,0:T(8,128)(2,1)}) %reduce-scatter.3.cloned.1.call-update) | async-done | bytes 393232 | tf_op jit(solution)/shard_map/reduce_scatter | solution.py:65
  150.8 1.8 add_convert_fusion.1
  152.8 0.7 all-gather.21.cloned.1.call-update
  153.5 0.7 all-gather.19.cloned.1.call-update
  154.3 0.7 all-gather.23.cloned.1.call-update
  155.1 0.7 slice_reduce_fusion.7
  155.7 16.7 %all-gather.17.cloned.1.call-done = bf16[384,2048]{1,0:T(8,128)(2,1)} async-done(((bf16[384,512]{1,0:T(8,128)(2,1)}), bf16[384,2048]{1,0:T(8,128)(2,1)}) %all-gather.17.cloned.1.call-update) | async-done | bytes 1572880 | tf_op jit(solution)/shard_map/all_gather | solution.py:69
  172.5 1.8 fusion.3
  174.3 97.8 %all-gather.21.cloned.1.call-done = bf16[2048,1280]{1,0:T(8,128)(2,1)} async-done(((bf16[512,1280]{1,0:T(8,128)(2,1)}), bf16[2048,1280]{1,0:T(8,128)(2,1)}) %all-gather.21.cloned.1.call-update) | async-done | bytes 5242896 | tf_op jit(solution)/shard_map/all_gather | solution.py:73
  272.1 5.2 %convolution_convert_fusion.1 = bf16[384,1280]{1,0:T(8,128)(2,1)S(1)} fusion(bf16[2048,1280]{1,0:T(8,128)(2,1)} %all-gather.21.cloned.1.call-done, bf16[384,2048]{1,0:T(8,128)(2,1)} %all-gather.17.cloned.1.call-done, f32[2048]{0:T(1024)S(1)} %copy-done.15, f32[384]{0:T(512)S(1)} %add_rsqrt_fusion), kind=kOutput, calls=%fused_computation.11 | convolution fusion | flops 2016903168 | bytes 7808512 | tf_op jit(solution)/shard_map/dot_general | solution.py:77
  277.5 92.6 %all-gather.19.cloned.1.call-done = bf16[2048,1280]{1,0:T(8,128)(2,1)} async-done(((bf16[512,1280]{1,0:T(8,128)(2,1)}), bf16[2048,1280]{1,0:T(8,128)(2,1)}) %all-gather.19.cloned.1.call-update) | async-done | bytes 5242896 | tf_op jit(solution)/shard_map/all_gather | solution.py:72
  370.1 4.8 convolution_convert_fusion.2
  375.6 1.2 fusion.8
  376.8 0.6 fusion.15
  377.4 90.7 %all-gather.23.cloned.1.call-done = bf16[1280,2048]{1,0:T(8,128)(2,1)} async-done(((bf16[1280,512]{1,0:T(8,128)(2,1)}), bf16[1280,2048]{1,0:T(8,128)(2,1)}) %all-gather.23.cloned.1.call-update) | async-done | bytes 5242896 | tf_op jit(solution)/shard_map/all_gather | solution.py:84
  468.1 5.9 %convolution_convert_fusion = bf16[384,2048]{1,0:T(8,128)(2,1)} fusion(bf16[384,1280]{1,0:T(8,128)(2,1)S(1)} %fusion.15, bf16[1280,2048]{1,0:T(8,128)(2,1)} %all-gather.23.cloned.1.call-done), kind=kOutput, calls=%fused_computation.10 | convolution fusion | flops 2014052352 | bytes 7798784 | tf_op jit(solution)/shard_map/dot_general | solution.py:83
  473.9 26.5 %reduce-scatter.5.cloned.1.call-done = bf16[384,512]{1,0:T(8,128)(2,1)} async-done(((bf16[384,2048]{1,0:T(8,128)(2,1)}), bf16[384,512]{1,0:T(8,128)(2,1)}) %reduce-scatter.5.cloned.1.call-update) | async-done | bytes 393232 | tf_op jit(solution)/shard_map/reduce_scatter | solution.py:86
  500.4 1.8 add_convert_fusion
  (53 shorter events, 2.0 us)
Async XLA Ops:
  6.5 24.7 %all-gather.9.cloned.1.call-start = ((), (), s32[]{:S(2)}) async-start(), calls=%async_computation.3 | async-start | bytes 1966080 | tf_op jit(solution)/shard_map/all_gather | solution.py:43
  7.3 53.6 %all-gather.13.cloned.1.call-start = ((), (), s32[]{:S(2)}) async-start(), calls=%async_computation.5 | async-start | bytes 1310720 | tf_op jit(solution)/shard_map/all_gather | solution.py:46
  8.0 9.8 %copy-start.12 = (f32[3,256]{1,0:T(4,128)S(1)}, f32[3,256]{1,0:T(4,128)}, u32[]{:S(2)}) copy-start(f32[3,256]{1,0:T(4,128)} %param.18) | copy-start | bytes 9220
  8.0 81.8 %all-gather.11.cloned.1.call-start = ((), (), s32[]{:S(2)}) async-start(), calls=%async_computation.4 | async-start | bytes 1310720 | tf_op jit(solution)/shard_map/all_gather | solution.py:47
  10.8 32.2 %copy-start.14 = (f32[2048]{0:T(1024)S(1)}, f32[2048]{0:T(1024)}, u32[]{:S(2)}) copy-start(f32[2048]{0:T(1024)} %param.14) | copy-start | bytes 24580
  10.8 32.2 %all-to-all-start = ((bf16[4,512,256]{2,1,0:T(8,128)(2,1)}), bf16[4,512,256]{2,1,0:T(8,128)(2,1)S(1)}, u32[]{:S(2)}, u32[]{:S(2)}) async-start(bf16[4,512,256]{2,1,0:T(8,128)(2,1)} %stack.2), calls=%async_computation | async-start | bytes 2097152 | tf_op jit(solution)/shard_map/all_to_all | solution.py:49
  17.2 101.4 %all-gather.15.cloned.1.call-start = ((), (), s32[]{:S(2)}) async-start(), calls=%async_computation.6 | async-start | bytes 1310720 | tf_op jit(solution)/shard_map/all_gather | solution.py:62
  17.8 133.0 %reduce-scatter.3.cloned.1.call-start = ((), (), s32[]{:S(2)}) async-start(), calls=%async_computation.7 | async-start | bytes 1966080 | tf_op jit(solution)/shard_map/reduce_scatter | solution.py:65
  43.0 17.9 %copy-start.1 = (bf16[384,2048]{1,0:T(8,128)(2,1)S(1)}, bf16[384,2048]{1,0:T(8,128)(2,1)}, u32[]{:S(2)}) copy-start(bf16[384,2048]{1,0:T(8,128)(2,1)} %all-gather.9.cloned.1.call-done) | copy-start | bytes 4718596
  118.6 32.2 %copy-start.3 = (bf16[384,512]{1,0:T(8,128)(2,1)S(1)}, bf16[384,512]{1,0:T(8,128)(2,1)}, u32[]{:S(2)}) copy-start(bf16[384,512]{1,0:T(8,128)(2,1)} %param.13) | copy-start | bytes 1179652
  123.3 49.2 %all-gather.17.cloned.1.call-start = ((), (), s32[]{:S(2)}) async-start(), calls=%async_computation.8 | async-start | bytes 1966080 | tf_op jit(solution)/shard_map/all_gather | solution.py:69
  152.7 2.3 copy-start.11
  152.7 2.4 copy-start.10
  152.7 119.4 %all-gather.21.cloned.1.call-start = ((), (), s32[]{:S(2)}) async-start(), calls=%async_computation.10 | async-start | bytes 6553600 | tf_op jit(solution)/shard_map/all_gather | solution.py:73
  153.5 118.7 %copy-start.15 = (f32[2048]{0:T(1024)S(1)}, f32[2048]{0:T(1024)}, u32[]{:S(2)}) copy-start(f32[2048]{0:T(1024)} %param.20) | copy-start | bytes 24580
  153.5 216.6 %all-gather.19.cloned.1.call-start = ((), (), s32[]{:S(2)}) async-start(), calls=%async_computation.9 | async-start | bytes 6553600 | tf_op jit(solution)/shard_map/all_gather | solution.py:72
  154.2 313.8 %all-gather.23.cloned.1.call-start = ((), (), s32[]{:S(2)}) async-start(), calls=%async_computation.11 | async-start | bytes 6553600 | tf_op jit(solution)/shard_map/all_gather | solution.py:84
  155.0 345.5 %reduce-scatter.5.cloned.1.call-start = ((), (), s32[]{:S(2)}) async-start(), calls=%async_computation.12 | async-start | bytes 1966080 | tf_op jit(solution)/shard_map/reduce_scatter | solution.py:86
  174.3 103.1 %copy-start.13 = (f32[384]{0:T(512)}, f32[384]{0:T(512)S(1)}, u32[]{:S(2)}) copy-start(f32[384]{0:T(512)S(1)} %add_rsqrt_fusion) | copy-start | bytes 4612
  277.4 92.7 %copy-start.2 = (bf16[384,2048]{1,0:T(8,128)(2,1)S(1)}, bf16[384,2048]{1,0:T(8,128)(2,1)}, u32[]{:S(2)}) copy-start(bf16[384,2048]{1,0:T(8,128)(2,1)} %all-gather.17.cloned.1.call-done) | copy-start | bytes 4718596
  374.8 0.7 copy-start.4
  374.8 0.7 copy-start.5
  374.9 0.7 copy-start.6
  374.9 0.7 copy-start.7
  374.9 0.7 copy-start.8
  374.9 0.7 copy-start.9
  377.4 123.1 %copy-start = (bf16[384,512]{1,0:T(8,128)(2,1)S(1)}, bf16[384,512]{1,0:T(8,128)(2,1)}, u32[]{:S(2)}) copy-start(bf16[384,512]{1,0:T(8,128)(2,1)} %add_convert_fusion.1) | copy-start | bytes 1179652
Sparse Core Ops, SparseCore 0:
  8.9 22.3 all-gather.8
  32.8 27.9 all-gather.12
  62.4 27.3 all-gather.10
  91.3 27.3 all-gather.14
  123.4 27.3 reduce-scatter.2
  152.8 19.6 all-gather.16
  174.0 98.0 all-gather.20
  273.7 96.3 all-gather.18
  371.7 96.3 all-gather.22
  474.1 26.3 reduce-scatter.4
